TPU v7x, 512 devices: a whole 4x4x16 slice. The times are simulated.
512 devices in a mesh: sp: 128 (over z, x, core), tp: 4 (over y).
Axes of the slice: x: 4, y: 4, z: 16, core: 2. Of those that a mesh axis runs over, the one named last changes fastest.
Arguments:
- tokens: bfloat16 [16384, 2048], P(('sp', 'tp')), may hold values from -6 to 6
- input_norm_gain: float32 [2048], replicated, may hold values from 0.1 to 1.9
- convolution_value_weight: bfloat16 [2048, 1024], P('sp', 'tp'), may hold values from -0.125 to 0.125
- convolution_gate_weight: bfloat16 [2048, 1024], P('sp', 'tp'), may hold values from -0.125 to 0.125
- depthwise_filter_taps: float32 [31, 1024], P(None, 'tp'), may hold values from -4 to 4
- channel_norm_gain: float32 [1024], P('tp'), may hold values from 0.1 to 1.9
- channel_norm_bias: float32 [1024], P('tp'), may hold values from -3 to 3
- query_projection_weight: bfloat16 [2048, 1024], P('sp', 'tp'), may hold values from -0.125 to 0.125
- forget_gate_weight: bfloat16 [2048, 1024], P('sp', 'tp'), may hold values from -0.125 to 0.125
- recurrence_value_weight: bfloat16 [2048, 1024], P('sp', 'tp'), may hold values from -0.125 to 0.125
- output_gate_weight: bfloat16 [2048, 1024], P('sp', 'tp'), may hold values from -0.125 to 0.125
- forget_floor_margin: float32 [1024], P('tp'), may hold values from 6.1035156e-06 to 0.1
- decay_jump_terms: float32 [8, 16384], P('tp', 'sp'), may hold values from -0.7 to 0
- head_norm_gain: float32 [1024], P('tp'), may hold values from 0.1 to 1.9
- convolution_output_weight: bfloat16 [1024, 2048], P('tp', 'sp'), may hold values from -0.125 to 0.125
- recurrence_output_weight: bfloat16 [1024, 2048], P('tp', 'sp'), may hold values from -0.125 to 0.125
Outputs:
- mixed: bfloat16 [16384, 2048], P(('sp', 'tp'))
All inputs are finite; a program needn't handle non-finite values.
Results may differ from a plain program's by a relative error of at most 0.015.
Values may be sent and summed in bfloat16 or wider, within the bound.
A program may use at most 64 MiB of HBM per device.

v0:
```python
import jax
import jax.numpy as jnp
from jax import lax
from jax.sharding import Mesh
from jax.sharding import PartitionSpec as P

CONV_CH = 1024
HG_DK = 128
HG_DV = 128
HG_BLOCK = 64
SP = ("sp_0", "sp_1", "sp_2")
SP_TP = ("sp_0", "sp_1", "sp_2", "tp")
norm_eps = 1e-06
layer_eps = 1e-05


def rows_first(arrays, axis, dims):
    turned = [jnp.moveaxis(a, dim, 0) for a, dim in zip(arrays, dims)]
    both = jnp.concatenate([t.reshape(len(t), -1) for t in turned], axis=1)
    out, at, outs = (lax.all_gather(both, axis, axis=0, tiled=True), 0, [])
    for t, dim in zip(turned, dims):
        section = out[:, at : at + t[0].size].reshape(-1, *t.shape[1:])
        outs.append(jnp.moveaxis(section, 0, dim))
        at += t[0].size
    return tuple(outs)


def joined_along(blocks, dim):
    shape = list(blocks.shape[1:])
    shape[dim] *= blocks.shape[0]
    return jnp.moveaxis(blocks, 0, dim).reshape(shape)


def sent_to_all(x, axis):
    copies = jnp.broadcast_to(x, (lax.axis_size(axis), *x.shape))
    return lax.all_to_all(copies, axis, split_axis=0, concat_axis=0, tiled=True)


def gather_directly(x, axis, dim):
    return joined_along(sent_to_all(x, axis), dim)


def passed_along(value, axis, steps):
    count = lax.axis_size(axis)
    initial, last = (max(0, -steps), min(count, count - steps))
    return lax.ppermute(value, axis, [(source, source + steps) for source in range(initial, last)])


def filled_with(x, identity):
    return jax.tree.map(
        lambda part, zero: jnp.zeros_like(part) + jnp.asarray(zero, part.dtype), x, identity
    )


def entering(x, axes, combine, identity):
    before = start = filled_with(x, identity)
    running = x
    for axis in reversed(axes):
        size, mine = (lax.axis_size(axis), lax.axis_index(axis))
        pieces = jax.tree.map(
            lambda part, kind: lax.all_gather(part.astype(kind), axis),
            running,
            (jnp.bfloat16, jnp.bfloat16),
        )
        inside, running = (start, start)
        for k in range(size):
            passed = k < mine
            running = combine(
                running, jax.tree.map(lambda part, own: part[k].astype(own.dtype), pieces, x)
            )
            inside = jax.tree.map(lambda new, old: jnp.where(passed, new, old), running, inside)
        before = combine(inside, before)
    return before


def of_everyone(x, axis):
    return sent_to_all(x, axis).sum(axis=0)


def together(arrays, axis):
    flat, at, outs = (jnp.concatenate([a.reshape(-1) for a in arrays]), 0, [])
    running = of_everyone(flat, axis)
    for a in arrays:
        outs.append(running[at : at + a.size].reshape(a.shape))
        at += a.size
    return tuple(outs)


def in_blocks(x, dim, size):
    shape = x.shape
    blocks = x.reshape(*shape[:dim], size, shape[dim] // size, *shape[dim + 1 :])
    return jnp.moveaxis(blocks, dim, 0)


def sent_and_summed(x, axis, dim):
    blocks = in_blocks(x, dim, lax.axis_size(axis))
    arrived = lax.all_to_all(blocks, axis, split_axis=0, concat_axis=0, tiled=True)
    return arrived.astype(jnp.float32).sum(axis=0)


def convolve(gated, kernel):
    return lax.conv_general_dilated(
        gated[None],
        kernel[:, None, :],
        (1,),
        "VALID",
        dimension_numbers=("NWC", "WIO", "NWC"),
        feature_group_count=gated.shape[1],
    )[0]


def channel_norm(values, first_sum, second_sum, gain, bias):
    mean_value = first_sum[:, None] / CONV_CH
    variance = second_sum[:, None] / CONV_CH - mean_value * mean_value
    shifted = (values - mean_value) * lax.rsqrt(variance + layer_eps) * gain + bias
    return jax.nn.silu(shifted).astype(jnp.bfloat16)


def gate_factors(query_projected, forget_projected, forget_floor_margin, decay_jump_rows):
    row_total_count = query_projected.shape[0]
    head_total_count = decay_jump_rows.shape[1]
    query_rows = jax.nn.silu(query_projected.astype(jnp.float32))
    log_forget_gate = jnp.logaddexp(
        jnp.log1p(-forget_floor_margin),
        jnp.log(forget_floor_margin) + jax.nn.log_sigmoid(forget_projected.astype(jnp.float32)),
    )
    key_gate_values = -jnp.expm1(log_forget_gate)
    log_decay_running = (
        log_forget_gate.reshape(row_total_count, head_total_count, -1) + decay_jump_rows[:, :, None]
    )
    return (
        query_rows.reshape(row_total_count, head_total_count, -1),
        key_gate_values.reshape(row_total_count, head_total_count, -1),
        log_decay_running,
    )


def finish(recurrent, gain, outgate_proj):
    row_total_count = recurrent.shape[0]
    scaled = recurrent * lax.rsqrt(
        jnp.mean(recurrent * recurrent, axis=2, keepdims=True) + norm_eps
    )
    gated_out = (
        scaled.reshape(row_total_count, -1) * gain * jax.nn.silu(outgate_proj.astype(jnp.float32))
    )
    return gated_out.astype(jnp.bfloat16)


def combine_states(first_part, second_part):
    return (
        first_part[0] + second_part[0],
        jnp.exp(second_part[0])[:, :, None] * first_part[1] + second_part[1],
    )


def carry_step(recurrence_state, block_parts):
    decay_end, contribution = block_parts
    return (jnp.exp(decay_end)[:, :, None] * recurrence_state + contribution, recurrence_state)


def per_device(
    tokens,
    input_norm_gain,
    convolution_value_weight,
    convolution_gate_weight,
    depthwise_filter_taps,
    channel_norm_gain,
    channel_norm_bias,
    query_projection_weight,
    forget_gate_weight,
    recurrence_value_weight,
    output_gate_weight,
    forget_floor_margin,
    decay_jump_terms,
    head_norm_gain,
    convolution_output_weight,
    recurrence_output_weight,
):
    features = tokens.astype(jnp.float32)
    normed = (
        features
        * lax.rsqrt(jnp.mean(features * features, axis=1, keepdims=True) + norm_eps)
        * input_norm_gain
    ).astype(jnp.bfloat16)
    gathered = rows_first(
        (
            convolution_value_weight,
            convolution_gate_weight,
            query_projection_weight,
            forget_gate_weight,
            recurrence_value_weight,
            output_gate_weight,
            convolution_output_weight,
            recurrence_output_weight,
        ),
        SP,
        (0, 0, 0, 0, 0, 0, 1, 1),
    )
    projection_weights = gathered[:6]
    conv_columns = gathered[6]
    rec_columns = gathered[7]

    def project(row_piece):
        return jnp.concatenate(
            [
                jnp.dot(row_piece, weight, preferred_element_type=jnp.float32).astype(jnp.bfloat16)
                for weight in projection_weights
            ],
            axis=1,
        )

    projected = project(gather_directly(normed, "tp", 0))
    offsets = []
    position = 0
    for weight in projection_weights[:-1]:
        position = position + weight.shape[1]
        offsets.append(position)
    value_proj, gate_proj, query_projected, forget_projected, input_proj, outgate_proj = jnp.split(
        projected, offsets, axis=1
    )
    row_total_count = value_proj.shape[0]
    rim_rows = depthwise_filter_taps.shape[0] - 1
    tail_value, tail_gate = passed_along(
        (value_proj[row_total_count - rim_rows :], gate_proj[row_total_count - rim_rows :]), SP, 1
    )
    value_ext = jnp.concatenate([tail_value, value_proj], axis=0)
    gate_ext = jnp.concatenate([tail_gate, gate_proj], axis=0)
    gated = value_ext.astype(jnp.float32) * jax.nn.sigmoid(gate_ext.astype(jnp.float32))
    convolved = convolve(gated, depthwise_filter_taps).astype(jnp.bfloat16)
    device_heads = decay_jump_terms.shape[0]
    query_rows, key_gate_values, log_decay_running = gate_factors(
        query_projected, forget_projected, forget_floor_margin, decay_jump_terms.T
    )
    input_rows = input_proj.astype(jnp.float32).reshape(row_total_count, device_heads, -1)
    block_count = row_total_count // HG_BLOCK

    def to_blocks(array):
        return array.reshape(block_count, HG_BLOCK, device_heads, -1).transpose(0, 2, 1, 3)

    block_queries = to_blocks(query_rows)
    block_keys = to_blocks(key_gate_values)
    block_inputs = to_blocks(input_rows)
    cumulative = jnp.cumsum(to_blocks(log_decay_running), axis=2)
    final_decay = cumulative[:, :, -1, :]
    query_rows_scaled = block_queries * jnp.exp(cumulative)
    scaled_keys = block_keys * jnp.exp(-cumulative)
    final_keys = block_keys * jnp.exp(final_decay[:, :, None, :] - cumulative)
    attention_scores = jnp.einsum("nhtk,nhsk->nhts", query_rows_scaled, scaled_keys)
    causal = jnp.arange(HG_BLOCK)[:, None] >= jnp.arange(HG_BLOCK)[None, :]
    attention_scores = jnp.where(causal[None, None], attention_scores, 0.0)
    inner = jnp.einsum("nhts,nhsv->nhtv", attention_scores, block_inputs)
    contributions = jnp.einsum("nhsk,nhsv->nhkv", final_keys, block_inputs)
    initial = jnp.zeros((device_heads, HG_DK, HG_DV), jnp.float32)
    local_state, block_starts = lax.scan(carry_step, initial, (final_decay, contributions))
    device_decay = jnp.sum(final_decay, axis=0)
    before_blocks = jnp.cumsum(final_decay, axis=0) - final_decay
    incoming = entering(
        (device_decay, local_state),
        SP,
        combine_states,
        (jnp.zeros_like(device_decay), jnp.zeros_like(local_state)),
    )
    starts = block_starts + jnp.exp(before_blocks)[:, :, :, None] * incoming[1][None]
    recurrent = inner + jnp.einsum("nhtk,nhkv->nhtv", query_rows_scaled, starts)
    recurrent = recurrent.transpose(0, 2, 1, 3).reshape(row_total_count, device_heads, -1)
    rec_out = finish(recurrent, head_norm_gain, outgate_proj)
    values = convolved.astype(jnp.float32)
    totals = together((jnp.sum(values, axis=1), jnp.sum(values * values, axis=1)), "tp")
    conv_out = channel_norm(values, totals[0], totals[1], channel_norm_gain, channel_norm_bias)
    conv_part = lax.slice_in_dim(
        conv_out, 0, row_total_count // lax.axis_size("tp") * lax.axis_size("tp"), axis=0
    )
    summed = sent_and_summed(
        (
            jnp.dot(conv_part, conv_columns, preferred_element_type=jnp.float32)
            + jnp.dot(rec_out, rec_columns, preferred_element_type=jnp.float32)
        ).astype(jnp.bfloat16),
        "tp",
        0,
    )
    return summed.astype(jnp.bfloat16)


def solution(mesh):
    split = Mesh(mesh.devices.reshape(16, 4, 2, mesh.shape["tp"]), ("sp_0", "sp_1", "sp_2", "tp"))
    return jax.shard_map(
        per_device,
        mesh=split,
        in_specs=(
            P(SP_TP, None),
            P(),
            P(SP, "tp"),
            P(SP, "tp"),
            P(None, "tp"),
            P("tp"),
            P("tp"),
            P(SP, "tp"),
            P(SP, "tp"),
            P(SP, "tp"),
            P(SP, "tp"),
            P("tp"),
            P("tp", SP),
            P("tp"),
            P("tp", SP),
            P("tp", SP),
        ),
        out_specs=P(SP_TP, None),
        check_vma=False,
    )
```

profile of v0, /device:TPU:6, one launch (start us, length us, event | category | flops | bytes accessed | tf_op | source)
XLA Modules:
  0.0 284.3 jit_solution(15545226052518464159)
XLA Ops:
  6.5 0.7 constant_dynamic-update-slice_fusion.7
  7.2 0.7 constant_dynamic-update-slice_fusion.6
  7.9 0.7 constant_dynamic-update-slice_fusion.5
  8.6 0.7 constant_dynamic-update-slice_fusion.4
  9.3 0.7 constant_dynamic-update-slice_fusion.3
  10.0 0.7 constant_dynamic-update-slice_fusion.2
  10.7 0.7 constant_dynamic-update-slice_fusion.1
  11.4 0.7 constant_dynamic-update-slice_fusion
  12.1 0.6 copy-done.1
  12.8 1.0 fusion.18
  13.8 1.0 fusion.20
  14.9 0.9 broadcast_in_dim.27
  15.8 4.5 %all-to-all-start = ((bf16[4,32,2048]{2,1,0:T(8,128)(2,1)}), bf16[4,32,2048]{2,1,0:T(8,128)(2,1)S(1)}, u32[]{:S(2)}, u32[]{:S(2)}) async-start(bf16[4,32,2048]{2,1,0:T(8,128)(2,1)} %broadcast_in_dim.27), calls=%async_computation | async-start | bytes 1048576 | tf_op jit(solution)/shard_map/all_to_all | solution.py:36
  20.2 0.8 add.274
  21.0 0.7 negate_log-plus-one_fusion
  21.7 8.0 %all-to-all-done = bf16[4,32,2048]{2,1,0:T(8,128)(2,1)S(1)} async-done(((bf16[4,32,2048]{2,1,0:T(8,128)(2,1)}), bf16[4,32,2048]{2,1,0:T(8,128)(2,1)S(1)}, u32[]{:S(2)}, u32[]{:S(2)}) %all-to-all-start) | async-done | bytes 524320 | tf_op jit(solution)/shard_map/all_to_all | solution.py:36
  29.7 132.8 %all-gather.6.cloned.1.call-done = bf16[2048,2048]{1,0:T(8,128)(2,1)} async-done(((bf16[16,2048]{1,0:T(8,128)(2,1)}), bf16[2048,2048]{1,0:T(8,128)(2,1)}) %all-gather.6.cloned.1.call-update) | async-done | bytes 8388624 | tf_op jit(solution)/shard_map/all_gather | solution.py:20
  162.5 1.7 exponential-minus-one_negate_fusion
  164.4 0.1 reduce_window_sum.22
  164.7 1.5 convolution_convert_fusion.2
  166.3 0.2 fusion.39
  166.5 0.4 while.13
  166.6 0.1 bitcast_add_fusion.2
  166.9 1.9 all-gather.1
  168.8 1.8 all-gather.2
  170.6 0.1 fusion.63
  170.8 12.3 %all_gather.35 = bf16[4,2,128,128]{3,2,1,0:T(8,128)(2,1)S(1)} all-gather(bf16[1,2,128,128]{3,2,1,0:T(8,128)(2,1)S(1)} %fusion.63), channel_id=1, replica_groups=mesh['sp_0'=16,'sp_1'=4,'sp_2'=2,'tp'=4] {'sp_1'}, dimensions={0}, use_global_device_ids=true | all-gather | bytes 327680 | tf_op jit(solution)/shard_map/all_gather | solution.py:61
  183.0 8.5 %all_gather.31 = bf16[4,2,128]{2,1,0:T(2,128)(2,1)S(1)} all-gather(bf16[1,2,128]{2,1,0:T(2,128)(2,1)S(1)} %get-tuple-element.87), channel_id=1, replica_groups=mesh['sp_0'=16,'sp_1'=4,'sp_2'=2,'tp'=4] {'sp_1'}, dimensions={0}, use_global_device_ids=true | all-gather | bytes 2560 | tf_op jit(solution)/shard_map/all_gather | solution.py:61
  191.5 0.8 fusion.46
  192.4 1.6 divide_multiply_fusion.1
  194.0 1.5 convolution_convert_fusion.6
  195.6 1.9 collective-permute-start
  197.5 1.5 convolution_convert_fusion.5
  199.1 4.9 %collective-permute-start.1 = (bf16[30,256]{1,0:T(8,128)(2,1)S(1)}, bf16[30,256]{1,0:T(8,128)(2,1)S(1)}, u32[]{:S(2)}, u32[]{:S(2)}) collective-permute-start(bf16[30,256]{1,0:T(8,128)(2,1)S(1)} %slice.237), channel_id=1, source_target_pairs={{0,4},{4,8},{8,12},{12,16},{16,20},{20,24},{24,28},{28,32},{32,36}... | collective-permute-start | bytes 46088 | tf_op jit(solution)/shard_map/ppermute | solution.py:46
  203.9 26.1 %all_gather.32 = bf16[16,2,128]{2,1,0:T(2,128)(2,1)S(1)} all-gather(bf16[1,2,128]{2,1,0:T(2,128)(2,1)S(1)} %get-tuple-element.83), channel_id=1, replica_groups=mesh['sp_0'=16,'sp_1'=4,'sp_2'=2,'tp'=4] {'sp_0'}, dimensions={0}, use_global_device_ids=true | all-gather | bytes 8704 | tf_op jit(solution)/shard_map/all_gather | solution.py:61
  230.0 0.3 fusion.2
  230.4 2.2 fusion.97
  232.8 0.6 broadcast_in_dim.29
  233.3 4.3 %all-to-all-start.1 = ((f32[4,1,256]{2,1,0:T(1,128)}), f32[4,1,256]{2,1,0:T(1,128)S(1)}, u32[]{:S(2)}, u32[]{:S(2)}) async-start(f32[4,1,256]{2,1,0:T(1,128)} %broadcast_in_dim.29), calls=%async_computation.1 | async-start | bytes 8192 | tf_op jit(solution)/shard_map/all_to_all | solution.py:36
  237.6 5.3 %all-to-all-done.1 = f32[4,1,256]{2,1,0:T(1,128)S(1)} async-done(((f32[4,1,256]{2,1,0:T(1,128)}), f32[4,1,256]{2,1,0:T(1,128)S(1)}, u32[]{:S(2)}, u32[]{:S(2)}) %all-to-all-start.1) | async-done | bytes 4128 | tf_op jit(solution)/shard_map/all_to_all | solution.py:36
  243.0 1.7 fusion.14
  244.7 14.4 %all-gather.8.cloned.1.call-done = bf16[16,2,128,128]{3,2,1,0:T(8,128)(2,1)} async-done(((bf16[1,2,128,128]{3,2,1,0:T(8,128)(2,1)}), bf16[16,2,128,128]{3,2,1,0:T(8,128)(2,1)}) %all-gather.8.cloned.1.call-update) | async-done | bytes 1048592 | tf_op jit(solution)/shard_map/all_gather | solution.py:61
  259.1 2.1 fusion.38
  261.2 0.4 multiply_reduce_fusion
  261.8 0.2 mul.422
  262.1 2.5 fusion
  264.5 12.2 %all_to_all.16 = bf16[4,32,2048]{2,1,0:T(8,128)(2,1)S(1)} all-to-all(bf16[4,32,2048]{2,1,0:T(8,128)(2,1)S(1)} %bitcast.162), channel_id=1, replica_groups=mesh['sp_0'=16,'sp_1'=4,'sp_2'=2,'tp'=4] {'tp'}, dimensions={0} | all-to-all | bytes 1048576 | tf_op jit(solution)/shard_map/all_to_all | solution.py:97
  276.7 0.7 reduce_sum.72
  (47 shorter events, 1.1 us)
Async XLA Ops:
  6.5 223.9 %copy-start = (f32[31,256]{1,0:T(8,128)S(1)}, f32[31,256]{1,0:T(8,128)}, u32[]{:S(2)}) copy-start(f32[31,256]{1,0:T(8,128)} %param.22) | copy-start | bytes 95236
  6.5 156.0 %all-gather.6.cloned.1.call-start = ((), (), s32[]{:S(2)}) async-start(), calls=%async_computation.3 | async-start | bytes 8454144 | tf_op jit(solution)/shard_map/all_gather | solution.py:20
  12.1 0.6 copy-start.1
  15.8 13.9 %all-to-all-start = ((bf16[4,32,2048]{2,1,0:T(8,128)(2,1)}), bf16[4,32,2048]{2,1,0:T(8,128)(2,1)S(1)}, u32[]{:S(2)}, u32[]{:S(2)}) async-start(bf16[4,32,2048]{2,1,0:T(8,128)(2,1)} %broadcast_in_dim.27), calls=%async_computation | async-start | bytes 1048576 | tf_op jit(solution)/shard_map/all_to_all | solution.py:36
  20.2 238.9 %all-gather.8.cloned.1.call-start = ((), (), s32[]{:S(2)}) async-start(), calls=%async_computation.4 | async-start | bytes 1114112 | tf_op jit(solution)/shard_map/all_gather | solution.py:61
  166.2 76.7 %copy-start.2 = (f32[256]{0:T(256)S(1)}, f32[256]{0:T(256)}, u32[]{:S(2)}) copy-start(f32[256]{0:T(256)} %param.24) | copy-start | bytes 3076
  166.2 76.7 %copy-start.3 = (f32[256]{0:T(256)S(1)}, f32[256]{0:T(256)}, u32[]{:S(2)}) copy-start(f32[256]{0:T(256)} %param.23) | copy-start | bytes 3076
  170.8 91.3 %copy-start.4 = (f32[256]{0:T(256)S(1)}, f32[256]{0:T(256)}, u32[]{:S(2)}) copy-start(f32[256]{0:T(256)} %param.31) | copy-start | bytes 3076
  195.6 34.7 %collective-permute-start = (bf16[30,256]{1,0:T(8,128)(2,1)S(1)}, bf16[30,256]{1,0:T(8,128)(2,1)S(1)}, u32[]{:S(2)}, u32[]{:S(2)}) collective-permute-start(bf16[30,256]{1,0:T(8,128)(2,1)S(1)} %slice.235), channel_id=1, source_target_pairs={{0,4},{4,8},{8,12},{12,16},{16,20},{20,24},{24,28},{28,32},{32,36}... | collective-permute-start | bytes 46088 | tf_op jit(solution)/shard_map/ppermute | solution.py:46
  199.1 31.3 %collective-permute-start.1 = (bf16[30,256]{1,0:T(8,128)(2,1)S(1)}, bf16[30,256]{1,0:T(8,128)(2,1)S(1)}, u32[]{:S(2)}, u32[]{:S(2)}) collective-permute-start(bf16[30,256]{1,0:T(8,128)(2,1)S(1)} %slice.237), channel_id=1, source_target_pairs={{0,4},{4,8},{8,12},{12,16},{16,20},{20,24},{24,28},{28,32},{32,36}... | collective-permute-start | bytes 46088 | tf_op jit(solution)/shard_map/ppermute | solution.py:46
  233.3 9.6 %all-to-all-start.1 = ((f32[4,1,256]{2,1,0:T(1,128)}), f32[4,1,256]{2,1,0:T(1,128)S(1)}, u32[]{:S(2)}, u32[]{:S(2)}) async-start(f32[4,1,256]{2,1,0:T(1,128)} %broadcast_in_dim.29), calls=%async_computation.1 | async-start | bytes 8192 | tf_op jit(solution)/shard_map/all_to_all | solution.py:36
Sparse Core Ops, SparseCore 0:
  12.9 149.5 all-gather.5
  192.5 66.5 all-gather.7
where the time goes:
time: 285 us; the launch traced here: 284 us
  waiting for transfers between devices  161 us (56%)
  blocking collectives  62.7 us (22%)
  starting transfers between devices  15.5 us (5%)
  matrix products  15.2 us (5%)
  between operations  13.7 us (5%)
  local copies, waits for them, and re-layouts  9.17 us (3%)
  other arithmetic  7.39 us (3%)
    all_gather x1, waiting for transfers between devices, rows_first(): out, at, outs = (lax.all_gather(both, axis, axis=0, tiled=True), 0, [])  133 us
    all_gather x5, blocking collectives, entering(): lax.all_gather(part.astype(kind), axis)  50.5 us
    all_gather x1, waiting for transfers between devices, entering(): lax.all_gather(part.astype(kind), axis)  14.4 us
    all_to_all x2, waiting for transfers between devices, sent_to_all(): return lax.all_to_all(copies, axis, split_axis=0, concat_axis=0, tiled=True)  13.3 us
    all_to_all x1, blocking collectives, sent_and_summed(): lax.all_to_all(blocks, axis, split_axis=0, concat_axis=0, tiled=True)  12.2 us
    all_to_all x2, starting transfers between devices, sent_to_all(): return lax.all_to_all(copies, axis, split_axis=0, concat_axis=0, tiled=True)  8.75 us
    dot_general x5, matrix products, project(): jnp.dot(row_piece, weight, preferred_element_type=jnp.float32)  7.87 us
    ppermute x2, starting transfers between devices, passed_along(): lax.ppermute(value, axis, [(source, source + steps) for source in range(i...  6.78 us
  transfers between devices with their start and end apart: 6, of which 4 were waited for; matrix products, arithmetic and copies ran while one was open for 5% of the time, Pallas kernels for 0%

commit v1 on v0

--- a/solution.py
+++ b/solution.py
@@ -17,7 +17,13 @@
 def rows_first(arrays, axis, dims):
     turned = [jnp.moveaxis(a, dim, 0) for a, dim in zip(arrays, dims)]
     both = jnp.concatenate([t.reshape(len(t), -1) for t in turned], axis=1)
-    out, at, outs = (lax.all_gather(both, axis, axis=0, tiled=True), 0, [])
+    out, at, outs = (
+        jnp.concatenate(
+            lax.all_to_all(jnp.stack([both] * lax.axis_size(axis)), axis, 0, 0), axis=0
+        ),
+        0,
+        [],
+    )
     for t, dim in zip(turned, dims):
         section = out[:, at : at + t[0].size].reshape(-1, *t.shape[1:])
         outs.append(jnp.moveaxis(section, 0, dim))

time: 285 us -> 537 us (1.88)
  waiting for transfers between devices: 161 us -> 385 us
  starting transfers between devices: 15.5 us -> 34.1 us
  blocking collectives: 62.7 us -> 68.5 us
    all_to_all x0 -> x1, waiting for transfers between devices: none -> 363 us  [rows_first(): lax.all_to_all(jnp.stack([both] * lax.axis_size(axis)), axis, 0, 0)]
    all_gather x1 -> x0, waiting for transfers between devices: 133 us -> none  [rows_first(): out, at, outs = (lax.all_gather(both, axis, axis=0, tiled=True), 0, [])]
    all_to_all x0 -> x1, starting transfers between devices: none -> 20 us  [rows_first(): lax.all_to_all(jnp.stack([both] * lax.axis_size(axis)), axis, 0, 0)]
    all_gather x5, blocking collectives: 50.5 us -> 56.3 us  [entering(): lax.all_gather(part.astype(kind), axis)]
  transfers between devices with their start and end apart: 6 -> 6, of which waited for: 4 -> 4; matrix products, arithmetic and copies ran while one was open for 5% -> 2% of each run, Pallas kernels for 0% -> 0%
where the time goes in v1:
time: 537 us; the launch traced here: 536 us
  waiting for transfers between devices  385 us (72%)
  blocking collectives  68.5 us (13%)
  starting transfers between devices  34.1 us (6%)
  matrix products  15.2 us (3%)
  between operations  13.8 us (3%)
  local copies, waits for them, and re-layouts  12.1 us (2%)
  other arithmetic  6.71 us (1%)
    all_to_all x1, waiting for transfers between devices, rows_first(): lax.all_to_all(jnp.stack([both] * lax.axis_size(axis)), axis, 0, 0)  363 us
    all_gather x5, blocking collectives, entering(): lax.all_gather(part.astype(kind), axis)  56.3 us
    all_to_all x1, starting transfers between devices, rows_first(): lax.all_to_all(jnp.stack([both] * lax.axis_size(axis)), axis, 0, 0)  20 us
    all_gather x1, waiting for transfers between devices, entering(): lax.all_gather(part.astype(kind), axis)  12.7 us
    all_to_all x1, blocking collectives, sent_and_summed(): lax.all_to_all(blocks, axis, split_axis=0, concat_axis=0, tiled=True)  12.2 us
  transfers between devices with their start and end apart: 6, of which 4 were waited for; matrix products, arithmetic and copies ran while one was open for 2% of the time, Pallas kernels for 0%

profile of v1, /device:TPU:6, one launch (start us, length us, event | category | flops | bytes accessed | tf_op | source)
XLA Modules:
  0.0 535.6 jit_solution(11815351215714003366)
XLA Ops:
  6.5 1.0 fusion.18
  7.6 1.0 fusion.20
  8.6 0.8 broadcast_in_dim.27
  9.4 4.5 all-to-all-start
  13.9 0.7 constant_dynamic-update-slice_fusion.7
  14.6 0.7 constant_dynamic-update-slice_fusion.6
  15.3 0.7 constant_dynamic-update-slice_fusion.5
  16.0 0.7 constant_dynamic-update-slice_fusion.4
  16.7 0.7 constant_dynamic-update-slice_fusion.3
  17.4 0.7 constant_dynamic-update-slice_fusion.2
  18.1 0.7 constant_dynamic-update-slice_fusion.1
  18.8 0.7 constant_dynamic-update-slice_fusion
  19.5 3.9 all-to-all-done
  23.4 4.3 stack.2
  27.7 20.0 %all-to-all-start.1 = ((bf16[128,16,2048]{2,1,0:T(8,128)(2,1)}), bf16[128,16,2048]{2,1,0:T(8,128)(2,1)}, u32[]{:S(2)}, u32[]{:S(2)}) async-start(bf16[128,16,2048]{2,1,0:T(8,128)(2,1)} %stack.2), calls=%async_computation.1 | async-start | bytes 16777216 | tf_op jit(solution)/shard_map/all_to_all | solution.py:22
  47.9 363.4 %all-to-all-done.1 = bf16[128,16,2048]{2,1,0:T(8,128)(2,1)} async-done(((bf16[128,16,2048]{2,1,0:T(8,128)(2,1)}), bf16[128,16,2048]{2,1,0:T(8,128)(2,1)}, u32[]{:S(2)}, u32[]{:S(2)}) %all-to-all-start.1) | async-done | bytes 8388640 | tf_op jit(solution)/shard_map/all_to_all | solution.py:22
  411.2 1.5 convolution_convert_fusion.2
  412.8 1.6 divide_multiply_fusion.1
  414.3 1.5 convolution_convert_fusion.6
  415.9 1.7 exponential-minus-one_negate_fusion
  417.8 0.1 reduce_window_sum.22
  418.1 0.2 fusion.39
  418.3 0.4 while.13
  418.4 0.1 bitcast_add_fusion.2
  418.6 0.1 bitcast_add_fusion.2
  418.7 1.9 all-gather.1
  420.6 1.8 all-gather.2
  422.4 0.1 fusion.63
  422.6 14.2 %all_gather.31 = bf16[4,2,128,128]{3,2,1,0:T(8,128)(2,1)S(1)} all-gather(bf16[1,2,128,128]{3,2,1,0:T(8,128)(2,1)S(1)} %fusion.63), channel_id=1, replica_groups=mesh['sp_0'=16,'sp_1'=4,'sp_2'=2,'tp'=4] {'sp_1'}, dimensions={0}, use_global_device_ids=true | all-gather | bytes 327680 | tf_op jit(solution)/shard_map/all_gather | solution.py:67
  436.8 9.1 %all_gather.27 = bf16[4,2,128]{2,1,0:T(2,128)(2,1)S(1)} all-gather(bf16[1,2,128]{2,1,0:T(2,128)(2,1)S(1)} %get-tuple-element.87), channel_id=1, replica_groups=mesh['sp_0'=16,'sp_1'=4,'sp_2'=2,'tp'=4] {'sp_1'}, dimensions={0}, use_global_device_ids=true | all-gather | bytes 2560 | tf_op jit(solution)/shard_map/all_gather | solution.py:67
  445.9 0.8 fusion.46
  446.9 1.9 collective-permute-start
  448.8 1.5 convolution_convert_fusion.5
  450.4 4.5 collective-permute-start.1
  454.9 29.3 %all_gather.28 = bf16[16,2,128]{2,1,0:T(2,128)(2,1)S(1)} all-gather(bf16[1,2,128]{2,1,0:T(2,128)(2,1)S(1)} %get-tuple-element.83), channel_id=1, replica_groups=mesh['sp_0'=16,'sp_1'=4,'sp_2'=2,'tp'=4] {'sp_0'}, dimensions={0}, use_global_device_ids=true | all-gather | bytes 8704 | tf_op jit(solution)/shard_map/all_gather | solution.py:67
  484.2 0.3 fusion.2
  484.6 2.2 fusion.97
  486.9 0.6 broadcast_in_dim.29
  487.5 3.2 all-to-all-start.2
  490.8 5.2 all-to-all-done.2
  496.1 1.7 fusion.14
  497.8 12.7 %all-gather.5.cloned.1.call-done = bf16[16,2,128,128]{3,2,1,0:T(8,128)(2,1)} async-done(((bf16[1,2,128,128]{3,2,1,0:T(8,128)(2,1)}), bf16[16,2,128,128]{3,2,1,0:T(8,128)(2,1)}) %all-gather.5.cloned.1.call-update) | async-done | bytes 1048592 | tf_op jit(solution)/shard_map/all_gather | solution.py:67
  510.5 2.1 fusion.38
  512.6 0.4 multiply_reduce_fusion
  513.2 0.2 mul.422
  513.4 2.5 fusion
  515.9 12.2 %all_to_all.21 = bf16[4,32,2048]{2,1,0:T(8,128)(2,1)S(1)} all-to-all(bf16[4,32,2048]{2,1,0:T(8,128)(2,1)S(1)} %bitcast.163), channel_id=1, replica_groups=mesh['sp_0'=16,'sp_1'=4,'sp_2'=2,'tp'=4] {'tp'}, dimensions={0} | all-to-all | bytes 1048576 | tf_op jit(solution)/shard_map/all_to_all | solution.py:103
  528.1 0.7 reduce_sum.72
  (49 shorter events, 1.1 us)
Async XLA Ops:
  6.5 478.0 %copy-start = (f32[31,256]{1,0:T(8,128)S(1)}, f32[31,256]{1,0:T(8,128)}, u32[]{:S(2)}) copy-start(f32[31,256]{1,0:T(8,128)} %param.22) | copy-start | bytes 95236
  9.4 13.9 %all-to-all-start = ((bf16[4,32,2048]{2,1,0:T(8,128)(2,1)}), bf16[4,32,2048]{2,1,0:T(8,128)(2,1)S(1)}, u32[]{:S(2)}, u32[]{:S(2)}) async-start(bf16[4,32,2048]{2,1,0:T(8,128)(2,1)} %broadcast_in_dim.27), calls=%async_computation | async-start | bytes 1048576 | tf_op jit(solution)/shard_map/all_to_all | solution.py:42
  27.7 20.1 %copy-start.4 = (f32[2,128]{1,0:T(2,128)S(1)}, f32[2,128]{1,0:T(2,128)}, u32[]{:S(2)}) copy-start(f32[2,128]{1,0:T(2,128)} %param.30) | copy-start | bytes 3076
  27.7 20.2 %copy-start.5 = (f32[256]{0:T(256)S(1)}, f32[256]{0:T(256)}, u32[]{:S(2)}) copy-start(f32[256]{0:T(256)} %param.29) | copy-start | bytes 3076
  27.7 383.6 %all-to-all-start.1 = ((bf16[128,16,2048]{2,1,0:T(8,128)(2,1)}), bf16[128,16,2048]{2,1,0:T(8,128)(2,1)}, u32[]{:S(2)}, u32[]{:S(2)}) async-start(bf16[128,16,2048]{2,1,0:T(8,128)(2,1)} %stack.2), calls=%async_computation.1 | async-start | bytes 16777216 | tf_op jit(solution)/shard_map/all_to_all | solution.py:22
  47.6 462.8 %all-gather.5.cloned.1.call-start = ((), (), s32[]{:S(2)}) async-start(), calls=%async_computation.4 | async-start | bytes 1114112 | tf_op jit(solution)/shard_map/all_gather | solution.py:67
  414.3 81.7 %copy-start.1 = (f32[256]{0:T(256)S(1)}, f32[256]{0:T(256)}, u32[]{:S(2)}) copy-start(f32[256]{0:T(256)} %param.24) | copy-start | bytes 3076
  414.3 81.7 %copy-start.2 = (f32[256]{0:T(256)S(1)}, f32[256]{0:T(256)}, u32[]{:S(2)}) copy-start(f32[256]{0:T(256)} %param.23) | copy-start | bytes 3076
  418.3 95.0 %copy-start.3 = (f32[256]{0:T(256)S(1)}, f32[256]{0:T(256)}, u32[]{:S(2)}) copy-start(f32[256]{0:T(256)} %param.31) | copy-start | bytes 3076
  446.9 37.6 %collective-permute-start = (bf16[30,256]{1,0:T(8,128)(2,1)S(1)}, bf16[30,256]{1,0:T(8,128)(2,1)S(1)}, u32[]{:S(2)}, u32[]{:S(2)}) collective-permute-start(bf16[30,256]{1,0:T(8,128)(2,1)S(1)} %slice.235), channel_id=1, source_target_pairs={{0,4},{4,8},{8,12},{12,16},{16,20},{20,24},{24,28},{28,32},{32,36}... | collective-permute-start | bytes 46088 | tf_op jit(solution)/shard_map/ppermute | solution.py:52
  450.4 34.1 %collective-permute-start.1 = (bf16[30,256]{1,0:T(8,128)(2,1)S(1)}, bf16[30,256]{1,0:T(8,128)(2,1)S(1)}, u32[]{:S(2)}, u32[]{:S(2)}) collective-permute-start(bf16[30,256]{1,0:T(8,128)(2,1)S(1)} %slice.237), channel_id=1, source_target_pairs={{0,4},{4,8},{8,12},{12,16},{16,20},{20,24},{24,28},{28,32},{32,36}... | collective-permute-start | bytes 46088 | tf_op jit(solution)/shard_map/ppermute | solution.py:52
  487.5 8.5 %all-to-all-start.2 = ((f32[4,1,256]{2,1,0:T(1,128)}), f32[4,1,256]{2,1,0:T(1,128)S(1)}, u32[]{:S(2)}, u32[]{:S(2)}) async-start(f32[4,1,256]{2,1,0:T(1,128)} %broadcast_in_dim.29), calls=%async_computation.2 | async-start | bytes 8192 | tf_op jit(solution)/shard_map/all_to_all | solution.py:42
Sparse Core Ops, SparseCore 0:
  446.9 63.5 all-gather.4
